TPU v7x, 32 devices: a whole 2x2x4 slice. The times are simulated.
32 devices in a mesh: sp: 4 (over x, core), tp: 8 (over z, y).
Axes of the slice: x: 2, y: 2, z: 4, core: 2. Of those that a mesh axis runs over, the one named last changes fastest.
Arguments:
- latents: bfloat16 [1024, 2048], P(('sp', 'tp')), may hold values from -6 to 6
- context: bfloat16 [256, 2048], P('sp'), may hold values from -6 to 6
- condition: float32 [2048], P('sp'), may hold values from -12 to 12
- context_condition: float32 [2048], P('sp'), may hold values from -12 to 12
- norm_gain: float32 [2048], replicated, may hold values from 0.1 to 1.9
- shift_weight: bfloat16 [2048, 2048], P('sp', 'tp'), may hold values from -0.09375 to 0.09375
- scale_weight: bfloat16 [2048, 2048], P('sp', 'tp'), may hold values from -0.09375 to 0.09375
- gate_weight: bfloat16 [2048, 2048], P('sp', 'tp'), may hold values from -0.125 to 0.125
- query_weight: bfloat16 [2048, 1024], P(None, 'tp'), may hold values from -0.125 to 0.125
- key_weight: bfloat16 [2048, 1024], P(None, 'tp'), may hold values from -0.125 to 0.125
- value_weight: bfloat16 [2048, 1024], P(None, 'tp'), may hold values from -0.125 to 0.125
- subtract_share: float32 [8], P('tp'), may hold values from 0.3 to 0.8
- head_gain: float32 [128], replicated, may hold values from 0.1 to 1.9
- output_weight: bfloat16 [1024, 2048], P('tp'), may hold values from -0.1875 to 0.1875
Outputs:
- updated: bfloat16 [1024, 2048], P(('sp', 'tp'))
All inputs are finite; a program needn't handle non-finite values.
Results may differ from a plain program's by a relative error of at most 0.013.
Values may be sent and summed in bfloat16 or wider, within the bound.
A program may use at most 64 MiB of HBM per device.

v0:
```python
import jax
import jax.numpy as jnp
from jax import lax
from jax.sharding import PartitionSpec as P

HEAD = 64
VALUE = 128
GRID_W = 64
norm_eps = 1e-06
head_eps = 1e-05
rope_theta = 10000.0
head_scale = 0.8


def rotary_tables(positions):
    quarter = HEAD // 4
    inverse = rope_theta ** (-2.0 * jnp.arange(quarter, dtype=jnp.float32) / (HEAD // 2))
    row_angle = (positions // GRID_W).astype(jnp.float32)[:, None] * inverse[None, :]
    column_angle = (positions % GRID_W).astype(jnp.float32)[:, None] * inverse[None, :]
    angles = jnp.concatenate([row_angle, row_angle, column_angle, column_angle], axis=-1)
    return (jnp.cos(angles), jnp.sin(angles))


def rotate(vectors, cosine, sine_table):
    quarter = HEAD // 4
    pieces = vectors.reshape(vectors.shape[:-1] + (2, 2, quarter))
    turned = jnp.concatenate([-pieces[..., 1:, :], pieces[..., :1, :]], axis=-2).reshape(
        vectors.shape
    )
    return vectors * cosine[:, None, :] + turned * sine_table[:, None, :]


def modulate(token_rows, gain_row, shift_row, scale_row):
    widened = token_rows.astype(jnp.float32)
    normed = widened * lax.rsqrt(jnp.mean(widened * widened, axis=-1, keepdims=True) + norm_eps)
    return (normed * gain_row * (1.0 + scale_row) + shift_row).astype(jnp.bfloat16)


def shards(
    latents,
    context,
    condition,
    context_condition,
    norm_gain,
    shift_weight,
    scale_weight,
    gate_weight,
    query_weight,
    key_weight,
    value_weight,
    subtract_share,
    head_gain,
    output_weight,
):
    activated = jax.nn.silu(jnp.stack([condition, context_condition])).astype(jnp.bfloat16)
    partial_terms = jnp.stack(
        [
            jnp.dot(activated, matrix, preferred_element_type=jnp.float32)
            for matrix in (shift_weight, scale_weight, gate_weight)
        ]
    )
    summed = lax.psum(partial_terms, "sp")
    full_terms = lax.all_gather(summed, "tp", axis=2, tiled=True)
    shift_terms, scale_terms, gate_terms = (full_terms[0], full_terms[1], full_terms[2])
    pair_weight = jnp.concatenate([key_weight, value_weight], axis=1)
    joined = jnp.concatenate([query_weight, pair_weight], axis=1)
    projected = jnp.dot(
        modulate(
            lax.all_gather(latents, "tp", axis=0, tiled=True),
            norm_gain,
            shift_terms[0],
            scale_terms[0],
        ),
        joined,
        preferred_element_type=jnp.float32,
    )
    local_count = projected.shape[0]
    positions = lax.axis_index("sp") * local_count + jnp.arange(local_count, dtype=jnp.int32)
    cosine, sine_table = rotary_tables(positions)
    queries = rotate(projected[:, :VALUE].reshape(local_count, 2, HEAD), cosine, sine_table)
    queries = queries.reshape(local_count, VALUE).astype(jnp.bfloat16)
    latent_keys = rotate(
        projected[:, VALUE : 2 * VALUE].reshape(local_count, 2, HEAD), cosine, sine_table
    )
    latent_keys = latent_keys.reshape(local_count, VALUE).astype(jnp.bfloat16)
    latent_pairs = jnp.concatenate(
        [latent_keys, projected[:, 2 * VALUE :].astype(jnp.bfloat16)], axis=1
    )
    context_mod = modulate(context, norm_gain, shift_terms[1], scale_terms[1])
    context_pairs = jnp.dot(context_mod, pair_weight, preferred_element_type=jnp.float32).astype(
        jnp.bfloat16
    )
    sent_pairs = jnp.concatenate([latent_pairs, context_pairs], axis=0)
    arrived = lax.all_gather(sent_pairs, "sp", axis=0, tiled=True)
    updated_carry = []
    for which_map in range(2):
        offset = which_map * HEAD
        scores = jnp.einsum(
            "qd,kd->qk",
            queries[:, offset : offset + HEAD],
            arrived[:, offset : offset + HEAD],
            preferred_element_type=jnp.float32,
        ) * HEAD ** (-0.5)
        powers = jnp.exp(scores)
        updated_carry.append(
            jnp.dot(
                powers.astype(jnp.bfloat16), arrived[:, VALUE:], preferred_element_type=jnp.float32
            )
        )
        updated_carry.append(jnp.sum(powers, axis=1, keepdims=True))
    first_sum, first_total, second_sum, second_total = tuple(updated_carry)
    share_value = subtract_share[0]
    difference = first_sum / first_total - share_value * (second_sum / second_total)
    normed = difference * lax.rsqrt(
        jnp.mean(difference * difference, axis=1, keepdims=True) + head_eps
    )
    head_output = (normed * head_gain * head_scale).astype(jnp.bfloat16)
    branch = lax.psum_scatter(
        jnp.dot(head_output, output_weight, preferred_element_type=jnp.float32),
        "tp",
        scatter_dimension=0,
        tiled=True,
    )
    return (latents.astype(jnp.float32) + gate_terms[0] * branch).astype(jnp.bfloat16)


def solution(mesh):
    in_specs = (
        P(("sp", "tp"), None),
        P("sp", None),
        P("sp"),
        P("sp"),
        P(),
        P("sp", "tp"),
        P("sp", "tp"),
        P("sp", "tp"),
        P(None, "tp"),
        P(None, "tp"),
        P(None, "tp"),
        P("tp"),
        P(),
        P("tp", None),
    )
    out_specs = P(("sp", "tp"), None)
    return jax.shard_map(shards, mesh=mesh, in_specs=in_specs, out_specs=out_specs, check_vma=False)
```

profile of v0, /device:TPU:0, one launch (start us, length us, event | category | flops | bytes accessed | tf_op | source)
XLA Modules:
  0.0 143.5 jit_solution(7154837675321998949)
XLA Ops:
  6.5 0.0 copy-start
  6.5 0.0 copy-start.2
  6.5 0.0 copy-start.4
  6.5 0.0 copy-start.5
  6.5 0.0 copy-start.7
  6.5 0.0 all-gather.2.cloned.1.call-start
  6.6 0.7 all-gather.2.cloned.1.call-update
  7.3 0.0 reduce-scatter.2.cloned.1.call-start
  8.0 0.1 broadcast_multiply_fusion.1
  8.1 0.1 fusion.46
  8.2 0.1 copy.15
  8.4 0.1 copy.18
  8.5 1.1 convolution_bitcast_fusion.1
  9.6 1.1 convolution_bitcast_fusion
  10.7 0.0 copy-start.6
  10.7 1.2 convolution_bitcast_fusion.2
  11.9 8.5 %psum.7 = f32[3,2,256]{2,1,0:T(2,128)S(1)} all-reduce(f32[3,2,256]{2,1,0:T(2,128)S(1)} %pad_maximum_fusion.4), channel_id=1, replica_groups=mesh['sp'=4,'tp'=8] {'sp'}, use_global_device_ids=true, to_apply=%region_0.1 | all-reduce | flops 1536 | bytes 12288 | tf_op jit(solution)/shard_map/psum | solution.py:62
  20.4 26.4 %all_gather.9 = f32[3,2,2048]{2,1,0:T(2,128)S(1)} all-gather(f32[3,2,256]{2,1,0:T(2,128)S(1)} %psum.7), channel_id=1, replica_groups=mesh['sp'=4,'tp'=8] {'tp'}, dimensions={2}, use_global_device_ids=true | all-gather | bytes 55296 | tf_op jit(solution)/shard_map/all_gather | solution.py:63
  46.9 0.0 copy-done.2
  46.9 0.2 fusion.25
  47.1 0.0 copy-done.4
  47.1 0.0 copy-done.5
  47.1 0.0 copy-done.7
  47.1 0.3 convolution_convert_fusion
  47.5 5.4 %all-gather.2.cloned.1.call-done = bf16[256,2048]{1,0:T(8,128)(2,1)} async-done(((bf16[32,2048]{1,0:T(8,128)(2,1)}), bf16[256,2048]{1,0:T(8,128)(2,1)}) %all-gather.2.cloned.1.call-update) | async-done | bytes 1048592 | tf_op jit(solution)/shard_map/all_gather | solution.py:69
  52.9 1.5 %fusion.2 = f32[256]{0:T(256)S(1)} fusion(bf16[256,2048]{1,0:T(8,128)(2,1)} %all-gather.2.cloned.1.call-done), kind=kLoop, calls=%fused_computation.6 | loop fusion | flops 1572608 | bytes 1049600 | tf_op jit(solution)/shard_map/reduce_sum | solution.py:35
  54.4 0.0 copy-done.6
  54.4 2.0 %fusion.7 = f32[256,384]{1,0:T(8,128)S(1)} fusion(bf16[2048,128]{1,0:T(8,128)(2,1)S(1)} %copy-done.4, bf16[2048,128]{1,0:T(8,128)(2,1)S(1)} %copy-done.5, bf16[2048,128]{1,0:T(8,128)(2,1)S(1)} %copy-done.6, bf16[256,2048]{1,0:T(8,128)(2,1)} %all-gather.2.cloned.1.call-done, f32[2048]{0:T(1024)S(1)} %bitcast.40, f32[2048]{0:T(1024)S(1)} %bitcast.41, ...), kind=kOutput, calls=%fused_computation.11 | convolution fusion | flops 410517504 | bytes 3040256 | tf_op jit(solution)/shard_map/dot_general | solution.py:67
  56.5 0.1 copy.16
  56.6 0.1 copy.17
  56.7 0.1 copy.20
  56.8 0.1 copy.21
  57.0 7.9 %all_gather.11 = bf16[1280,256]{1,0:T(8,128)(2,1)S(1)} all-gather(bf16[320,256]{1,0:T(8,128)(2,1)S(1)} %pad_maximum_fusion), channel_id=1, replica_groups=mesh['sp'=4,'tp'=8] {'sp'}, dimensions={0}, use_global_device_ids=true | all-gather | bytes 819200 | tf_op jit(solution)/shard_map/all_gather | solution.py:94
  64.9 0.5 fusion.59
  65.4 0.0 copy-start.3
  65.5 0.5 fusion.60
  65.9 0.4 fusion.14
  66.3 0.4 multiply_reduce_fusion
  66.7 0.0 copy-done
  66.7 0.0 copy-done.3
  66.7 0.0 copy-start.1
  66.8 1.9 %fusion.39 = f32[256,2048]{1,0:T(8,128)} fusion(bf16[128,2048]{1,0:T(8,128)(2,1)S(1)} %copy-done, f32[256,128]{0,1:T(8,128)S(1)} %get-tuple-element.27, f32[128]{0:T(128)S(1)} %copy-done.3, f32[256]{0:T(256)S(1)} %add_rsqrt_fusion), kind=kOutput, calls=%fused_computation.58 | convolution fusion | flops 134348800 | bytes 2754048 | tf_op jit(solution)/shard_map/dot_general | solution.py:119
  68.6 0.0 reduce-scatter.2.cloned.1.call-update
  68.6 66.4 %reduce-scatter.2.cloned.1.call-done = f32[32,2048]{1,0:T(8,128)} async-done(((f32[256,2048]{1,0:T(8,128)}), f32[32,2048]{1,0:T(8,128)}) %reduce-scatter.2.cloned.1.call-update) | async-done | bytes 262160 | tf_op jit(solution)/shard_map/reduce_scatter | solution.py:118
  135.0 0.0 copy-done.1
  135.0 1.6 %add_convert_fusion = bf16[32,2048]{1,0:T(8,128)(2,1)} fusion(f32[32,2048]{1,0:T(8,128)} %reduce-scatter.2.cloned.1.call-done, bf16[32,2048]{1,0:T(8,128)(2,1)S(1)} %copy-done.1, f32[2048]{0:T(1024)S(1)} %bitcast.33), kind=kLoop, calls=%fused_computation.45 | loop fusion | flops 262144 | bytes 532480 | tf_op jit(solution)/shard_map/convert_element_type | solution.py:124
  (17 shorter events, 0.2 us)
Async XLA Ops:
  6.5 60.2 %copy-start = (bf16[128,2048]{1,0:T(8,128)(2,1)S(1)}, bf16[128,2048]{1,0:T(8,128)(2,1)}, u32[]{:S(2)}) copy-start(bf16[128,2048]{1,0:T(8,128)(2,1)} %param.27) | copy-start | bytes 1572868
  6.5 40.4 %copy-start.2 = (bf16[64,2048]{1,0:T(8,128)(2,1)S(1)}, bf16[64,2048]{1,0:T(8,128)(2,1)}, u32[]{:S(2)}) copy-start(bf16[64,2048]{1,0:T(8,128)(2,1)} %param.15) | copy-start | bytes 786436
  6.5 40.6 %copy-start.4 = (bf16[2048,128]{1,0:T(8,128)(2,1)S(1)}, bf16[2048,128]{1,0:T(8,128)(2,1)}, u32[]{:S(2)}) copy-start(bf16[2048,128]{1,0:T(8,128)(2,1)} %param.24) | copy-start | bytes 1572868
  6.5 40.6 %copy-start.5 = (bf16[2048,128]{1,0:T(8,128)(2,1)S(1)}, bf16[2048,128]{1,0:T(8,128)(2,1)}, u32[]{:S(2)}) copy-start(bf16[2048,128]{1,0:T(8,128)(2,1)} %param.23) | copy-start | bytes 1572868
  6.5 40.6 %copy-start.7 = (f32[2048]{0:T(1024)S(1)}, f32[2048]{0:T(1024)}, u32[]{:S(2)}) copy-start(f32[2048]{0:T(1024)} %param.18) | copy-start | bytes 24580
  6.5 46.3 %all-gather.2.cloned.1.call-start = ((), (), s32[]{:S(2)}) async-start(), calls=%async_computation.1 | async-start | bytes 1179648 | tf_op jit(solution)/shard_map/all_gather | solution.py:69
  7.3 127.7 %reduce-scatter.2.cloned.1.call-start = ((), (), s32[]{:S(2)}) async-start(), calls=%async_computation.2 | async-start | bytes 2359296 | tf_op jit(solution)/shard_map/reduce_scatter | solution.py:118
  10.7 43.7 %copy-start.6 = (bf16[2048,128]{1,0:T(8,128)(2,1)S(1)}, bf16[2048,128]{1,0:T(8,128)(2,1)}, u32[]{:S(2)}) copy-start(bf16[2048,128]{1,0:T(8,128)(2,1)} %param.22) | copy-start | bytes 1572868
  65.4 1.3 copy-start.3
  66.7 68.3 %copy-start.1 = (bf16[32,2048]{1,0:T(8,128)(2,1)S(1)}, bf16[32,2048]{1,0:T(8,128)(2,1)}, u32[]{:S(2)}) copy-start(bf16[32,2048]{1,0:T(8,128)(2,1)} %param.14) | copy-start | bytes 393220
Sparse Core Ops, SparseCore 0:
  9.5 43.3 all-gather.1
  68.8 66.2 reduce-scatter.1
where the time goes:
time: 144 us; the launch traced here: 143 us
  waiting for transfers between devices  72.5 us (50%)
  blocking collectives  42.9 us (30%)
  between operations  14.3 us (10%)
  matrix products  9.42 us (7%)
  other arithmetic  3.7 us (3%)
    reduce_scatter x1, waiting for transfers between devices, shards(): lax.psum_scatter(jnp.dot(head_output, output_weight, preferred_element_ty...  66.4 us
    all_gather x1, blocking collectives, shards(): full_terms = lax.all_gather(summed, 'tp', axis=2, tiled=True)  26.4 us
    psum x1, blocking collectives, shards(): summed = lax.psum(partial_terms, 'sp')  8.51 us
    all_gather x1, blocking collectives, shards(): arrived = lax.all_gather(sent_pairs, 'sp', axis=0, tiled=True)  7.9 us
    all_gather x1, waiting for transfers between devices, shards(): lax.all_gather(latents, 'tp', axis=0, tiled=True)  5.4 us
    dot_general x3, matrix products, shards(): jnp.dot(activated, matrix, preferred_element_type=jnp.float32)  3.45 us
  transfers between devices with their start and end apart: 2, of which 2 were waited for; matrix products, arithmetic and copies ran while one was open for 3% of the time, Pallas kernels for 0%

commit v1 on v0

--- a/solution.py
+++ b/solution.py
@@ -91,7 +91,12 @@
         jnp.bfloat16
     )
     sent_pairs = jnp.concatenate([latent_pairs, context_pairs], axis=0)
-    arrived = lax.all_gather(sent_pairs, "sp", axis=0, tiled=True)
+    ring = [sent_pairs]
+    for hop in range(3):
+        ring.append(lax.ppermute(ring[-1], "sp", [(dev, (dev + 1) % 4) for dev in range(4)]))
+    arrived = jnp.roll(
+        jnp.concatenate(ring[::-1], axis=0), (lax.axis_index("sp") + 1) * ring[0].shape[0], axis=0
+    )
     updated_carry = []
     for which_map in range(2):
         offset = which_map * HEAD

time: 144 us -> 151 us (1.049)
  waiting for transfers between devices: 72.5 us -> 89.1 us
  blocking collectives: 42.9 us -> 35.2 us
  matrix products: 9.42 us -> 7.83 us
    ppermute x0 -> x3, waiting for transfers between devices: none -> 13.6 us  [shards(): lax.ppermute(ring[-1], 'sp', [(dev, (dev + 1) % 4) for dev in range(4)])]
    all_gather x1 -> x0, blocking collectives: 7.9 us -> none  [shards(): arrived = lax.all_gather(sent_pairs, 'sp', axis=0, tiled=True)]
    all_gather x1, waiting for transfers between devices: 5.4 us -> 7.8 us  [shards(): lax.all_gather(latents, 'tp', axis=0, tiled=True)]
    dot_general x3, matrix products: 3.45 us -> 1.43 us  [shards(): jnp.dot(activated, matrix, preferred_element_type=jnp.float32)]
  transfers between devices with their start and end apart: 2 -> 5, of which waited for: 2 -> 5; matrix products, arithmetic and copies ran while one was open for 3% -> 2% of each run, Pallas kernels for 0% -> 0%
where the time goes in v1:
time: 151 us
  waiting for transfers between devices  89.1 us (59%)
  blocking collectives  35.2 us (23%)
  between operations  14.5 us (10%)
  matrix products  7.83 us (5%)
  other arithmetic  3.75 us (2%)
    reduce_scatter x1, waiting for transfers between devices, shards(): lax.psum_scatter(jnp.dot(head_output, output_weight, preferred_element_ty...  67 us
    all_gather x1, blocking collectives, shards(): full_terms = lax.all_gather(summed, 'tp', axis=2, tiled=True)  26.7 us
    ppermute x3, waiting for transfers between devices, shards(): lax.ppermute(ring[-1], 'sp', [(dev, (dev + 1) % 4) for dev in range(4)])  13.6 us
    psum x1, blocking collectives, shards(): summed = lax.psum(partial_terms, 'sp')  8.5 us
    all_gather x1, waiting for transfers between devices, shards(): lax.all_gather(latents, 'tp', axis=0, tiled=True)  7.8 us
  transfers between devices with their start and end apart: 5, of which 5 were waited for; matrix products, arithmetic and copies ran while one was open for 2% of the time, Pallas kernels for 0%

profile of v1, /device:TPU:0, one launch (start us, length us, event | category | flops | bytes accessed | tf_op | source)
XLA Modules:
  0.0 151.2 jit_solution(8445394811532671346)
XLA Ops:
  6.5 0.0 copy-start
  6.5 0.0 copy-start.4
  6.6 0.0 copy-start.11
  6.6 0.0 copy-start.9
  6.6 0.0 copy-start.8
  6.6 0.0 all-gather.2.cloned.1.call-start
  6.6 0.7 all-gather.2.cloned.1.call-update
  7.3 0.0 reduce-scatter.2.cloned.1.call-start
  7.4 0.1 broadcast_multiply_fusion.1
  7.5 0.1 fusion.48
  7.6 0.1 copy.15
  7.8 0.1 copy.18
  7.9 1.1 convolution_bitcast_fusion
  9.0 0.0 copy-done.6
  9.0 0.0 copy-done.5
  9.0 0.0 copy-done.2
  9.0 0.1 convolution_bitcast_fusion.1
  9.1 0.0 copy-done.3
  9.2 0.1 convolution_bitcast_fusion.2
  9.3 8.5 %psum.7 = f32[3,2,256]{2,1,0:T(2,128)S(1)} all-reduce(f32[3,2,256]{2,1,0:T(2,128)S(1)} %pad_maximum_fusion.5), channel_id=1, replica_groups=mesh['sp'=4,'tp'=8] {'sp'}, use_global_device_ids=true, to_apply=%region_0.1 | all-reduce | flops 1536 | bytes 12288 | tf_op jit(solution)/shard_map/psum | solution.py:62
  17.8 26.7 %all_gather.6 = f32[3,2,2048]{2,1,0:T(2,128)S(1)} all-gather(f32[3,2,256]{2,1,0:T(2,128)S(1)} %psum.7), channel_id=1, replica_groups=mesh['sp'=4,'tp'=8] {'tp'}, dimensions={2}, use_global_device_ids=true | all-gather | bytes 55296 | tf_op jit(solution)/shard_map/all_gather | solution.py:63
  44.5 0.0 copy-done.4
  44.5 0.2 fusion.25
  44.7 0.0 copy-start.10
  44.8 0.3 convolution_convert_fusion
  45.1 7.8 %all-gather.2.cloned.1.call-done = bf16[256,2048]{1,0:T(8,128)(2,1)} async-done(((bf16[32,2048]{1,0:T(8,128)(2,1)}), bf16[256,2048]{1,0:T(8,128)(2,1)}) %all-gather.2.cloned.1.call-update) | async-done | bytes 1048592 | tf_op jit(solution)/shard_map/all_gather | solution.py:69
  52.9 1.5 fusion.2
  54.4 2.0 %fusion.7 = f32[256,384]{1,0:T(8,128)S(1)} fusion(bf16[2048,128]{1,0:T(8,128)(2,1)S(1)} %copy-done.8, bf16[2048,128]{1,0:T(8,128)(2,1)S(1)} %copy-done.9, bf16[2048,128]{1,0:T(8,128)(2,1)S(1)} %copy-done.10, bf16[256,2048]{1,0:T(8,128)(2,1)} %all-gather.2.cloned.1.call-done, f32[2048]{0:T(1024)S(1)} %bitcast.40, f32[2048]{0:T(1024)S(1)} %bitcast.41, ...), kind=kOutput, calls=%fused_computation.11 | convolution fusion | flops 410517504 | bytes 3040256 | tf_op jit(solution)/shard_map/dot_general | solution.py:67
  56.5 0.1 copy.20
  56.7 0.1 copy.21
  56.8 0.1 copy.16
  56.9 0.1 copy.17
  57.1 0.1 collective-permute-start
  57.1 4.7 %collective-permute-done = bf16[320,256]{1,0:T(8,128)(2,1)S(1)} collective-permute-done((bf16[320,256]{1,0:T(8,128)(2,1)S(1)}, bf16[320,256]{1,0:T(8,128)(2,1)S(1)}, u32[]{:S(2)}, u32[]{:S(2)}) %collective-permute-start) | collective-permute-done | bytes 163872 | tf_op jit(solution)/shard_map/ppermute | solution.py:96
  61.9 0.0 collective-permute-start.1
  61.9 4.7 %collective-permute-done.1 = bf16[320,256]{1,0:T(8,128)(2,1)S(1)} collective-permute-done((bf16[320,256]{1,0:T(8,128)(2,1)S(1)}, bf16[320,256]{1,0:T(8,128)(2,1)S(1)}, u32[]{:S(2)}, u32[]{:S(2)}) %collective-permute-start.1) | collective-permute-done | bytes 163872 | tf_op jit(solution)/shard_map/ppermute | solution.py:96
  66.6 0.0 collective-permute-start.2
  67.3 4.1 %collective-permute-done.2 = bf16[320,256]{1,0:T(8,128)(2,1)S(1)} collective-permute-done((bf16[320,256]{1,0:T(8,128)(2,1)S(1)}, bf16[320,256]{1,0:T(8,128)(2,1)S(1)}, u32[]{:S(2)}, u32[]{:S(2)}) %collective-permute-start.2) | collective-permute-done | bytes 163872 | tf_op jit(solution)/shard_map/ppermute | solution.py:96
  71.6 0.5 fusion.63
  72.0 0.5 fusion.62
  72.5 0.0 copy-start.7
  72.6 0.5 fusion.14
  73.1 0.6 multiply_reduce_fusion
  73.8 1.9 %fusion.41 = f32[256,2048]{1,0:T(8,128)} fusion(bf16[128,2048]{1,0:T(8,128)(2,1)S(1)} %copy-done, f32[256,128]{0,1:T(8,128)S(1)} %get-tuple-element.27, f32[128]{0:T(128)S(1)} %copy-done.7, f32[256]{0:T(256)S(1)} %add_rsqrt_fusion), kind=kOutput, calls=%fused_computation.61 | convolution fusion | flops 134348800 | bytes 2754048 | tf_op jit(solution)/shard_map/dot_general | solution.py:124
  75.6 0.0 reduce-scatter.2.cloned.1.call-update
  75.7 67.0 %reduce-scatter.2.cloned.1.call-done = f32[32,2048]{1,0:T(8,128)} async-done(((f32[256,2048]{1,0:T(8,128)}), f32[32,2048]{1,0:T(8,128)}) %reduce-scatter.2.cloned.1.call-update) | async-done | bytes 262160 | tf_op jit(solution)/shard_map/reduce_scatter | solution.py:123
  142.7 0.0 copy-done.1
  142.7 1.6 %add_convert_fusion = bf16[32,2048]{1,0:T(8,128)(2,1)} fusion(f32[32,2048]{1,0:T(8,128)} %reduce-scatter.2.cloned.1.call-done, bf16[32,2048]{1,0:T(8,128)(2,1)S(1)} %copy-done.1, f32[2048]{0:T(1024)S(1)} %bitcast.33), kind=kLoop, calls=%fused_computation.45 | loop fusion | flops 262144 | bytes 532480 | tf_op jit(solution)/shard_map/convert_element_type | solution.py:129
  (38 shorter events, 0.4 us)
Async XLA Ops:
  6.5 67.2 %copy-start = (bf16[128,2048]{1,0:T(8,128)(2,1)S(1)}, bf16[128,2048]{1,0:T(8,128)(2,1)}, u32[]{:S(2)}) copy-start(bf16[128,2048]{1,0:T(8,128)(2,1)} %param.27) | copy-start | bytes 1572868
  6.5 2.5 %copy-start.6 = (f32[512]{0:T(512)S(1)}, f32[512]{0:T(512)}, u32[]{:S(2)}) copy-start(f32[512]{0:T(512)} %param.16) | copy-start | bytes 6148
  6.5 2.5 %copy-start.5 = (f32[512]{0:T(512)S(1)}, f32[512]{0:T(512)}, u32[]{:S(2)}) copy-start(f32[512]{0:T(512)} %param.17) | copy-start | bytes 6148
  6.5 2.5 %copy-start.2 = (bf16[512,256]{1,0:T(8,128)(2,1)S(1)}, bf16[512,256]{1,0:T(8,128)(2,1)}, u32[]{:S(2)}) copy-start(bf16[512,256]{1,0:T(8,128)(2,1)} %param.20) | copy-start | bytes 786436
  6.5 2.6 %copy-start.3 = (bf16[512,256]{1,0:T(8,128)(2,1)S(1)}, bf16[512,256]{1,0:T(8,128)(2,1)}, u32[]{:S(2)}) copy-start(bf16[512,256]{1,0:T(8,128)(2,1)} %param.19) | copy-start | bytes 786436
  6.5 38.0 %copy-start.4 = (bf16[64,2048]{1,0:T(8,128)(2,1)S(1)}, bf16[64,2048]{1,0:T(8,128)(2,1)}, u32[]{:S(2)}) copy-start(bf16[64,2048]{1,0:T(8,128)(2,1)} %param.15) | copy-start | bytes 786436
  6.6 38.2 %copy-start.11 = (f32[2048]{0:T(1024)S(1)}, f32[2048]{0:T(1024)}, u32[]{:S(2)}) copy-start(f32[2048]{0:T(1024)} %param.18) | copy-start | bytes 24580
  6.6 38.2 %copy-start.9 = (bf16[2048,128]{1,0:T(8,128)(2,1)S(1)}, bf16[2048,128]{1,0:T(8,128)(2,1)}, u32[]{:S(2)}) copy-start(bf16[2048,128]{1,0:T(8,128)(2,1)} %param.23) | copy-start | bytes 1572868
  6.6 38.2 %copy-start.8 = (bf16[2048,128]{1,0:T(8,128)(2,1)S(1)}, bf16[2048,128]{1,0:T(8,128)(2,1)}, u32[]{:S(2)}) copy-start(bf16[2048,128]{1,0:T(8,128)(2,1)} %param.24) | copy-start | bytes 1572868
  6.6 46.3 %all-gather.2.cloned.1.call-start = ((), (), s32[]{:S(2)}) async-start(), calls=%async_computation.1 | async-start | bytes 1179648 | tf_op jit(solution)/shard_map/all_gather | solution.py:69
  7.3 135.3 %reduce-scatter.2.cloned.1.call-start = ((), (), s32[]{:S(2)}) async-start(), calls=%async_computation.2 | async-start | bytes 2359296 | tf_op jit(solution)/shard_map/reduce_scatter | solution.py:123
  44.7 9.7 %copy-start.10 = (bf16[2048,128]{1,0:T(8,128)(2,1)S(1)}, bf16[2048,128]{1,0:T(8,128)(2,1)}, u32[]{:S(2)}) copy-start(bf16[2048,128]{1,0:T(8,128)(2,1)} %param.22) | copy-start | bytes 1572868
  57.1 4.8 %collective-permute-start = (bf16[320,256]{1,0:T(8,128)(2,1)S(1)}, bf16[320,256]{1,0:T(8,128)(2,1)S(1)}, u32[]{:S(2)}, u32[]{:S(2)}) collective-permute-start(bf16[320,256]{1,0:T(8,128)(2,1)S(1)} %pad_maximum_fusion), channel_id=1, source_target_pairs={{0,8},{8,16},{16,24},{24,0},{1,9},{9,17},{17,25},{25,1},{2,10},{10... | collective-permute-start | bytes 491528 | tf_op jit(solution)/shard_map/ppermute | solution.py:96
  61.9 4.7 %collective-permute-start.1 = (bf16[320,256]{1,0:T(8,128)(2,1)S(1)}, bf16[320,256]{1,0:T(8,128)(2,1)S(1)}, u32[]{:S(2)}, u32[]{:S(2)}) collective-permute-start(bf16[320,256]{1,0:T(8,128)(2,1)S(1)} %collective-permute-done), channel_id=1, source_target_pairs={{0,8},{8,16},{16,24},{24,0},{1,9},{9,17},{17,25},{25,1},{2,10},{10... | collective-permute-start | bytes 491528 | tf_op jit(solution)/shard_map/ppermute | solution.py:96
  66.6 4.7 %collective-permute-start.2 = (bf16[320,256]{1,0:T(8,128)(2,1)S(1)}, bf16[320,256]{1,0:T(8,128)(2,1)S(1)}, u32[]{:S(2)}, u32[]{:S(2)}) collective-permute-start(bf16[320,256]{1,0:T(8,128)(2,1)S(1)} %collective-permute-done.1), channel_id=1, source_target_pairs={{0,8},{8,16},{16,24},{24,0},{1,9},{9,17},{17,25},{25,1},{2,10},{10... | collective-permute-start | bytes 491528 | tf_op jit(solution)/shard_map/ppermute | solution.py:96
  72.5 1.2 copy-start.7
  75.6 67.0 %copy-start.1 = (bf16[32,2048]{1,0:T(8,128)(2,1)S(1)}, bf16[32,2048]{1,0:T(8,128)(2,1)}, u32[]{:S(2)}) copy-start(bf16[32,2048]{1,0:T(8,128)(2,1)} %param.14) | copy-start | bytes 393220
Sparse Core Ops, SparseCore 0:
  9.5 43.3 all-gather.1
  75.8 66.8 reduce-scatter.1
